TPU v7x, 32 devices: a whole 2x2x4 slice. The times are simulated.
32 devices in a mesh: ep: 8 (over z, x), tp: 4 (over y, core).
Axes of the slice: x: 2, y: 2, z: 4, core: 2. Of those that a mesh axis runs over, the one named last changes fastest.
Arguments:
- tokens: bfloat16 [32, 2048], P('ep'), may hold values from -6 to 6
- norm_gain: bfloat16 [2048], replicated, may hold values from 0.099609375 to 1.8984375
- in_weight: bfloat16 [2048, 1024], P(None, 'tp'), may hold values from -0.125 to 0.125
- decay_rate: float32 [64, 64], P('tp'), may hold values from 0.05 to 1
- frequency: float32 [64, 64], P('tp'), may hold values from -3 to 3
- log_step: float32 [64], P('tp'), may hold values from -2.3 to 0.7
- input_real: float32 [64, 64, 16], P('tp'), may hold values from -1.75 to 1.75
- input_imag: float32 [64, 64, 16], P('tp'), may hold values from -1.75 to 1.75
- output_real: float32 [64, 16, 64], P('tp'), may hold values from -0.5 to 0.5
- output_imag: float32 [64, 16, 64], P('tp'), may hold values from -0.5 to 0.5
- skip_gain: float32 [1024], P('tp'), may hold values from -3 to 3
- state_real: float32 [32, 64, 64], P('ep', 'tp'), may hold values from -6 to 6
- state_imag: float32 [32, 64, 64], P('ep', 'tp'), may hold values from -6 to 6
- out_weight: bfloat16 [1024, 2048], P('tp'), may hold values from -0.1875 to 0.1875
- ffn_gain: bfloat16 [2048], replicated, may hold values from 0.099609375 to 1.8984375
- expert_ids: int32 [32, 2], replicated, may hold values from 0 to 7, all different within a row; in each aligned block of 4 rows (0 to 3, 4 to 7, ...) at most 2 rows name the same one
- route_weights: float32 [32, 2], P('ep'), may hold values from 0.2 to 1
- gate_weight: bfloat16 [2048, 65536], P(None, ('ep', 'tp')), may hold values from -0.125 to 0.125
- up_weight: bfloat16 [2048, 65536], P(None, ('ep', 'tp')), may hold values from -0.125 to 0.125
- down_weight: bfloat16 [65536, 2048], P('ep', 'tp'), may hold values from -0.0625 to 0.0625
Outputs:
- mixed: bfloat16 [32, 2048], P('ep', 'tp')
- new_real: float32 [32, 64, 64], P('ep', 'tp')
- new_imag: float32 [32, 64, 64], P('ep', 'tp')
Inputs may be any that keep to these rules, and one draw needn't show every extreme that they name: `expert_ids`: the 2 experts of a row differ. In each aligned block of 4 rows (the rows of one index of ep) no expert is named by more than 2 rows, and in some blocks one expert is named by exactly 2 rows.
All inputs are finite; a program needn't handle non-finite values.
Results may differ from a plain program's by a relative error of at most 0.007.
Values may be sent and summed in bfloat16 or wider, within the bound.
A program may use at most 64 MiB of HBM per device.

v0:
```python
import jax
import jax.numpy as jnp
from jax import lax
from jax.sharding import PartitionSpec as P

EXPERTS = 8
EPSILON = 1e-06


def rms_scale(values, gain):
    floats = values.astype(jnp.float32)
    return (
        floats
        * lax.rsqrt(jnp.mean(floats * floats, axis=-1, keepdims=True) + EPSILON)
        * gain.astype(jnp.float32)
    )


def discretize(decay_rate, frequency, log_step, input_real, input_imag):
    step_size = jnp.exp(log_step)[:, None]
    lam_real = -decay_rate
    magnitude = jnp.exp(lam_real * step_size)
    turned = frequency * step_size
    bar_real = magnitude * jnp.cos(turned)
    bar_imag = magnitude * jnp.sin(turned)
    denom = lam_real * lam_real + frequency * frequency
    minus_one = bar_real - 1.0
    factor_real = (minus_one * lam_real + bar_imag * frequency) / denom
    factor_imag = (bar_imag * lam_real - minus_one * frequency) / denom
    b_real = factor_real[..., None] * input_real - factor_imag[..., None] * input_imag
    b_imag = factor_real[..., None] * input_imag + factor_imag[..., None] * input_real
    return (bar_real, bar_imag, b_real, b_imag)


def state_update(
    projected,
    state_real,
    state_imag,
    decay_rate,
    frequency,
    log_step,
    input_real,
    input_imag,
    output_real,
    output_imag,
    skip_gain,
):
    bar_real, bar_imag, b_real, b_imag = discretize(
        decay_rate, frequency, log_step, input_real, input_imag
    )
    count, groups, _ = state_real.shape
    high = lax.Precision.HIGHEST
    grouped = projected.astype(jnp.float32).reshape(count, groups, -1)
    drive_real = jnp.einsum("sgp,gnp->sgn", grouped, b_real, precision=high)
    drive_imag = jnp.einsum("sgp,gnp->sgn", grouped, b_imag, precision=high)
    new_real = bar_real * state_real - bar_imag * state_imag + drive_real
    new_imag = bar_real * state_imag + bar_imag * state_real + drive_imag
    readout = jnp.einsum("sgn,gpn->sgp", new_real, output_real, precision=high) - jnp.einsum(
        "sgn,gpn->sgp", new_imag, output_imag, precision=high
    )
    readout = readout.reshape(count, -1) + skip_gain * grouped.reshape(count, -1)
    return (jax.nn.gelu(readout).astype(jnp.bfloat16), new_real, new_imag)


def slot_table(own_ids, own_weights, slot_count):
    expert_range = jnp.arange(EXPERTS, dtype=jnp.int32)
    onehot = (own_ids[:, :, None] == expert_range).astype(jnp.int32)
    flat = onehot.reshape(-1, EXPERTS)
    before = (jnp.cumsum(flat, axis=0) - flat).reshape(onehot.shape)
    slots = jnp.arange(slot_count, dtype=jnp.int32)
    match = (before[..., None] == slots) & (onehot[..., None] > 0)
    table = jnp.sum(jnp.where(match, own_weights[:, :, None, None], 0.0), axis=1)
    return jnp.transpose(table, (1, 2, 0))


def shards(
    tokens,
    norm_gain,
    in_weight,
    decay_rate,
    frequency,
    log_step,
    input_real,
    input_imag,
    output_real,
    output_imag,
    skip_gain,
    state_real,
    state_imag,
    out_weight,
    ffn_gain,
    expert_ids,
    route_weights,
    gate_weight,
    up_weight,
    down_weight,
):
    normed_in = rms_scale(tokens, norm_gain).astype(jnp.bfloat16)
    projected = jnp.dot(normed_in, in_weight, preferred_element_type=jnp.float32).astype(
        jnp.bfloat16
    )
    activated, new_real, new_imag = state_update(
        projected,
        state_real,
        state_imag,
        decay_rate,
        frequency,
        log_step,
        input_real,
        input_imag,
        output_real,
        output_imag,
        skip_gain,
    )
    delta = lax.psum(jnp.dot(activated, out_weight, preferred_element_type=jnp.float32), "tp")
    hidden_state = (tokens.astype(jnp.float32) + delta).astype(jnp.bfloat16)
    normed = rms_scale(hidden_state, ffn_gain).astype(jnp.bfloat16)
    seq_count, width = normed.shape
    slot_count = seq_count // 2
    group_span = lax.axis_size("ep") // EXPERTS
    my_index = lax.axis_index("ep")
    own_ids = lax.dynamic_slice_in_dim(expert_ids, my_index * seq_count, seq_count, 0)
    unit_weights = jnp.ones(own_ids.shape, jnp.float32)
    select = slot_table(own_ids, unit_weights, slot_count)
    outgoing = jnp.einsum(
        "xcs,sd->xcd", select.astype(jnp.bfloat16), normed, preferred_element_type=jnp.float32
    ).astype(jnp.bfloat16)
    received = lax.all_to_all(
        jnp.repeat(outgoing, group_span, axis=0), "ep", split_axis=0, concat_axis=0, tiled=True
    )
    slot_rows = received.reshape(-1, width)
    gate_pre = jnp.dot(slot_rows, gate_weight, preferred_element_type=jnp.float32)
    up_pre = jnp.dot(slot_rows, up_weight, preferred_element_type=jnp.float32)
    hidden = (jax.nn.silu(gate_pre) * up_pre).astype(jnp.bfloat16)
    quarter = down_weight.shape[1]
    partial_out = jnp.dot(
        lax.all_gather(hidden, "tp", axis=1, tiled=True),
        down_weight,
        preferred_element_type=jnp.float32,
    )
    rounded = partial_out.astype(jnp.bfloat16).reshape(-1, slot_count, quarter)
    returned = lax.all_to_all(rounded, "ep", split_axis=0, concat_axis=0, tiled=True)
    summed = (
        returned.astype(jnp.float32).reshape(EXPERTS, group_span, slot_count, quarter).sum(axis=1)
    )
    weight_table = slot_table(own_ids, route_weights, slot_count)
    routed = jnp.einsum("xcs,xcd->sd", weight_table, summed, precision=lax.Precision.HIGHEST)
    residual = lax.dynamic_slice_in_dim(hidden_state, lax.axis_index("tp") * quarter, quarter, 1)
    mixed = (residual.astype(jnp.float32) + routed).astype(jnp.bfloat16)
    return (mixed, new_real, new_imag)


def solution(mesh):
    in_specs = (
        P("ep", None),
        P(),
        P(None, "tp"),
        P("tp", None),
        P("tp", None),
        P("tp"),
        P("tp", None, None),
        P("tp", None, None),
        P("tp", None, None),
        P("tp", None, None),
        P("tp"),
        P("ep", "tp", None),
        P("ep", "tp", None),
        P("tp", None),
        P(),
        P(),
        P("ep", None),
        P(None, ("ep", "tp")),
        P(None, ("ep", "tp")),
        P("ep", "tp"),
    )
    out_specs = (P("ep", "tp"), P("ep", "tp", None), P("ep", "tp", None))
    return jax.shard_map(shards, mesh=mesh, in_specs=in_specs, out_specs=out_specs, check_vma=False)
```

profile of v0, /device:TPU:0, one launch (start us, length us, event | category | flops | bytes accessed | tf_op | source)
XLA Modules:
  0.0 71.3 jit_solution(13652618909060821899)
XLA Ops:
  0.6 0.0 copy-start
  0.7 0.8 %constant_dynamic-slice_fusion = s32[4,2]{0,1:T(2,128)S(1)} fusion(s32[32,2]{0,1:T(2,128)} %param.35, s32[]{:T(128)S(6)} %select_n.14), kind=kLoop, calls=%fused_computation.78 | loop fusion | bytes 68 | tf_op jit(solution)/shard_map/dynamic_slice | solution.py:122
  1.5 0.1 copy.71
  1.6 0.1 eq.56
  1.7 0.1 fusion.42
  1.7 0.7 exp.10
  2.4 0.9 %fusion.19 = f32[4]{0:T(128)S(1)} fusion(bf16[4,2048]{1,0:T(4,128)(2,1)} %param.20), kind=kLoop, calls=%fused_computation.32 | loop fusion | flops 24572 | bytes 16400 | tf_op jit(solution)/shard_map/reduce_sum | solution.py:14
  3.3 0.7 convert_element_type.68
  4.0 1.5 %convolution_convert_fusion.2 = bf16[4,256]{1,0:T(4,128)(2,1)S(1)} fusion(bf16[2048,256]{1,0:T(8,128)(2,1)} %param.22, bf16[4,2048]{1,0:T(4,128)(2,1)} %param.20, f32[2048]{0:T(1024)S(1)} %convert_element_type.68, f32[4]{0:T(128)S(1)} %add_rsqrt_fusion.1), kind=kOutput, calls=%fused_computation.13 | convolution fusion | flops 4228096 | bytes 1075216 | tf_op jit(solution)/shard_map/dot_general | solution.py:99
  5.5 0.1 reshape.72
  5.6 0.8 %cosine_multiply_fusion = (f32[16,64]{1,0:T(8,128)S(1)}, f32[16,64]{1,0:T(8,128)S(1)}, f32[16,64]{1,0:T(8,128)S(1)}, f32[16,64]{1,0:T(8,128)S(1)}) fusion(f32[16,64]{1,0:T(8,128)} %param.24, f32[16,64]{1,0:T(8,128)} %param.23, f32[16]{0:T(128)S(1)} %exp.10), kind=kLoop, calls=%fused_computation.51 | loop fusion | flops 17408 | bytes 24640 | tf_op jit(solution)/shard_map/mul | solution.py:24
  6.4 1.2 %fusion.2 = f32[4,16,64]{2,0,1:T(4,128)S(1)} fusion(f32[16,64,16]{1,2,0:T(8,128)} %param.26, f32[16,64,16]{1,2,0:T(8,128)} %param.27, f32[16,64]{1,0:T(8,128)S(1)} %get-tuple-element.21, f32[16,64]{1,0:T(8,128)S(1)} %get-tuple-element.20, f32[4,16,64]{2,1,0:T(8,128)} %param.32, f32[4,16,64]{2,1,0:T(8,128)} %param.31, f32[16,64]{1,0:T(8,128)S(1)} %get-tuple-element.22, ...), kind=kOutput, calls=%fused_computation.6 | convolution fusion | flops 851968 | bytes 198656 | tf_op jit(solution)/shard_map/sgp,gnp->sgn/dot_general | solution.py:55
  7.6 1.2 %fusion.3 = f32[4,16,64]{2,0,1:T(4,128)S(1)} fusion(f32[16,64,16]{1,2,0:T(8,128)} %param.27, f32[16,64,16]{1,2,0:T(8,128)} %param.26, f32[16,64]{1,0:T(8,128)S(1)} %get-tuple-element.21, f32[16,64]{1,0:T(8,128)S(1)} %get-tuple-element.20, f32[4,16,64]{2,1,0:T(8,128)} %param.32, f32[4,16,64]{2,1,0:T(8,128)} %param.31, f32[16,64]{1,0:T(8,128)S(1)} %get-tuple-element.22, ...), kind=kOutput, calls=%fused_computation.8 | convolution fusion | flops 851968 | bytes 198656 | tf_op jit(solution)/shard_map/sgp,gnp->sgn/dot_general | solution.py:54
  8.8 0.1 fusion.45
  8.9 0.1 fusion.43
  9.0 0.7 convert_element_type.80
  9.7 1.2 %fusion.60 = f32[16,4,16]{2,1,0:T(4,128)S(1)} fusion(f32[4,16,64]{2,0,1:T(4,128)S(1)} %fusion.3, f32[16,16,64]{2,1,0:T(8,128)} %param.28), kind=kOutput, calls=%fused_computation.84 | convolution fusion | flops 786432 | bytes 86016 | tf_op jit(solution)/shard_map/sgn,gpn->sgp/dot_general | solution.py:58
  10.9 1.2 %fusion.1 = f32[4,16,16]{2,0,1:T(4,128)S(1)} fusion(f32[16,4,16]{2,1,0:T(4,128)S(1)} %fusion.60, f32[4,16,64]{2,0,1:T(4,128)S(1)} %fusion.2, f32[16,16,64]{2,1,0:T(8,128)} %param.29), kind=kOutput, calls=%fused_computation.4 | convolution fusion | flops 787456 | bytes 90112 | tf_op jit(solution)/shard_map/sgn,gpn->sgp/dot_general | solution.py:58
  12.1 0.1 reshape.73
  12.2 0.0 copy-done
  12.2 0.9 %fusion.46 = f32[4,2048]{1,0:T(4,128)S(1)} fusion(bf16[256,2048]{1,0:T(8,128)(2,1)S(1)} %copy-done, f32[4,256]{1,0:T(4,128)S(1)} %reshape.73, bf16[4,256]{1,0:T(4,128)(2,1)S(1)} %convolution_convert_fusion.2, f32[256]{0:T(256)} %param.30), kind=kOutput, calls=%fused_computation.69 | convolution fusion | flops 4206592 | bytes 1088512 | tf_op jit(solution)/shard_map/dot_general | solution.py:115
  13.2 12.9 %psum.7 = f32[4,2048]{1,0:T(4,128)S(1)} all-reduce(f32[4,2048]{1,0:T(4,128)S(1)} %fusion.46), channel_id=1, replica_groups=mesh['ep'=8,'tp'=4] {'tp'}, use_global_device_ids=true, to_apply=%region_1.0 | all-reduce | flops 8192 | bytes 65536 | tf_op jit(solution)/shard_map/psum | solution.py:115
  26.1 0.9 %fusion.16 = (f32[4]{0:T(128)S(1)}, bf16[4,2048]{1,0:T(4,128)(2,1)S(1)}) fusion(f32[4,2048]{1,0:T(4,128)S(1)} %psum.7, bf16[4,2048]{1,0:T(4,128)(2,1)} %param.20), kind=kLoop, calls=%fused_computation.29 | loop fusion | flops 49148 | bytes 65552 | tf_op jit(solution)/shard_map/reduce_sum | solution.py:14
  26.9 0.8 %select_reduce_fusion.1 = (f32[4,8,2]{1,0,2:T(4,128)S(1)}, bf16[4,8,2]{1,0,2:T(4,128)(2,1)S(1)}) fusion(f32[4,2]{0,1:T(2,128)} %param.36, s32[4,2,8]{2,0,1:T(4,128)S(1)} %copy.73, pred[4,2,8]{2,0,1:T(4,128)(4,1)S(1)} %copy.74), kind=kLoop, calls=%fused_computation.45 | loop fusion | flops 640 | bytes 736 | tf_op jit(solution)/shard_map/reduce_sum | solution.py:72
  27.7 0.2 convolution_convert_fusion
  27.9 0.1 copy.75
  28.0 12.5 %all_to_all.10 = bf16[8,2,2048]{2,1,0:T(2,128)(2,1)S(1)} all-to-all(bf16[8,2,2048]{2,1,0:T(2,128)(2,1)S(1)} %copy.75), channel_id=1, replica_groups=mesh['ep'=8,'tp'=4] {'ep'}, dimensions={0} | all-to-all | bytes 131072 | tf_op jit(solution)/shard_map/all_to_all | solution.py:128
  40.5 4.6 %fusion.61 = f32[16,2048]{1,0:T(8,128)S(1)} fusion(bf16[16,2048]{1,0:T(8,128)(2,1)S(1)} %reshape.74, bf16[2048,2048]{1,0:T(8,128)(2,1)} %param.37), kind=kOutput, calls=%fused_computation.85 | convolution fusion | flops 134217728 | bytes 8585216 | tf_op jit(solution)/shard_map/dot_general | solution.py:132
  45.1 4.6 %fusion = bf16[16,2048]{1,0:T(8,128)(2,1)S(1)} fusion(bf16[16,2048]{1,0:T(8,128)(2,1)S(1)} %reshape.74, bf16[2048,2048]{1,0:T(8,128)(2,1)} %param.38, f32[16,2048]{1,0:T(8,128)S(1)} %fusion.61), kind=kOutput, calls=%fused_computation.2 | convolution fusion | flops 134414336 | bytes 8650752 | tf_op jit(solution)/shard_map/dot_general | solution.py:133
  49.7 5.8 %all_gather.3 = bf16[16,8192]{1,0:T(8,128)(2,1)S(1)} all-gather(bf16[16,2048]{1,0:T(8,128)(2,1)S(1)} %fusion), channel_id=1, replica_groups=mesh['ep'=8,'tp'=4] {'tp'}, dimensions={1}, use_global_device_ids=true | all-gather | bytes 327680 | tf_op jit(solution)/shard_map/all_gather | solution.py:137
  55.5 4.6 %convolution_convert_fusion.1 = bf16[16,512]{1,0:T(8,128)(2,1)S(1)} fusion(bf16[16,8192]{1,0:T(8,128)(2,1)S(1)} %all_gather.3, bf16[8192,512]{1,0:T(8,128)(2,1)} %param.39), kind=kOutput, calls=%fused_computation.9 | convolution fusion | flops 134225920 | bytes 8667136 | tf_op jit(solution)/shard_map/dot_general | solution.py:136
  60.0 0.6 reshape.75
  60.7 3.3 %all-to-all-start.1 = ((bf16[8,2,512]{2,1,0:T(2,128)(2,1)}), bf16[8,2,512]{2,1,0:T(2,128)(2,1)S(1)}, u32[]{:S(2)}, u32[]{:S(2)}) async-start(bf16[8,2,512]{2,1,0:T(2,128)(2,1)} %reshape.75), calls=%async_computation.1 | async-start | bytes 32768 | tf_op jit(solution)/shard_map/all_to_all | solution.py:142
  64.0 0.6 copy.77
  64.6 0.6 copy.78
  65.2 5.3 %all-to-all-done.1 = bf16[8,2,512]{2,1,0:T(2,128)(2,1)S(1)} async-done(((bf16[8,2,512]{2,1,0:T(2,128)(2,1)}), bf16[8,2,512]{2,1,0:T(2,128)(2,1)S(1)}, u32[]{:S(2)}, u32[]{:S(2)}) %all-to-all-start.1) | async-done | bytes 16416 | tf_op jit(solution)/shard_map/all_to_all | solution.py:142
  70.5 0.8 %fusion.5 = bf16[4,512]{1,0:T(4,128)(2,1)} fusion(bf16[8,2,512]{2,1,0:T(2,128)(2,1)S(1)} %all-to-all-done.1, f32[4,8,2]{1,0,2:T(4,128)S(1)} %get-tuple-element.15, bf16[4,2048]{1,0:T(4,128)(2,1)S(1)} %get-tuple-element.18, s32[]{:T(128)S(6)} %select_n.13), kind=kOutput, calls=%fused_computation.12 | convolution fusion | flops 399360 | bytes 24836 | tf_op jit(solution)/shard_map/xcs,xcd->sd/dot_general | solution.py:147
  (7 shorter events, 0.1 us)
Async XLA Ops:
  0.6 11.6 %copy-start = (bf16[256,2048]{1,0:T(8,128)(2,1)S(1)}, bf16[256,2048]{1,0:T(8,128)(2,1)}, u32[]{:S(2)}) copy-start(bf16[256,2048]{1,0:T(8,128)(2,1)} %param.33) | copy-start | bytes 3145732
  60.7 9.9 %all-to-all-start.1 = ((bf16[8,2,512]{2,1,0:T(2,128)(2,1)}), bf16[8,2,512]{2,1,0:T(2,128)(2,1)S(1)}, u32[]{:S(2)}, u32[]{:S(2)}) async-start(bf16[8,2,512]{2,1,0:T(2,128)(2,1)} %reshape.75), calls=%async_computation.1 | async-start | bytes 32768 | tf_op jit(solution)/shard_map/all_to_all | solution.py:142
where the time goes:
time: 72.1 us; the launch traced here: 71.3 us
  blocking collectives  31.2 us (43%)
  matrix products  22 us (31%)
  waiting for transfers between devices  5.28 us (7%)
  other arithmetic  4.97 us (7%)
  local copies, waits for them, and re-layouts  3.84 us (5%)
  starting transfers between devices  3.33 us (5%)
  between operations  0.73 us (1%)
    psum x1, blocking collectives, shards(): lax.psum(jnp.dot(activated, out_weight, preferred_element_type=jnp.float3...  12.9 us
    all_to_all x1, blocking collectives, shards(): lax.all_to_all(jnp.repeat(outgoing, group_span, axis=0), 'ep', split_axis...  12.5 us
    all_gather x1, blocking collectives, shards(): lax.all_gather(hidden, 'tp', axis=1, tiled=True)  5.77 us
    all_to_all x1, waiting for transfers between devices, shards(): lax.all_to_all(rounded, 'ep', split_axis=0, concat_axis=0, tiled=True)  5.28 us
    dot_general x1, matrix products, shards(): up_pre = jnp.dot(slot_rows, up_weight, preferred_element_type=jnp.float32)  4.58 us
    dot_general x1, matrix products, shards(): jnp.dot(slot_rows, gate_weight, preferred_element_type=jnp.float32)  4.58 us
    dot_general x1, matrix products, shards(): jnp.dot(lax.all_gather(hidden, 'tp', axis=1, tiled=True), down_weight, pr...  4.56 us
    all_to_all x1, starting transfers between devices, shards(): lax.all_to_all(rounded, 'ep', split_axis=0, concat_axis=0, tiled=True)  3.33 us
  transfers between devices with their start and end apart: 1, of which 1 were waited for; matrix products, arithmetic and copies ran while one was open for 2% of the time, Pallas kernels for 0%

commit v1 on v0

--- a/solution.py
+++ b/solution.py
@@ -112,7 +112,10 @@
         output_imag,
         skip_gain,
     )
-    delta = lax.psum(jnp.dot(activated, out_weight, preferred_element_type=jnp.float32), "tp")
+    delta = jnp.sum(
+        lax.all_gather(jnp.dot(activated, out_weight, preferred_element_type=jnp.float32), "tp"),
+        axis=0,
+    )
     hidden_state = (tokens.astype(jnp.float32) + delta).astype(jnp.bfloat16)
     normed = rms_scale(hidden_state, ffn_gain).astype(jnp.bfloat16)
     seq_count, width = normed.shape

time: 72.1 us -> 66 us (0.915)
  blocking collectives: 31.2 us -> 25.2 us
    psum x1 -> x0, blocking collectives: 12.9 us -> none  [shards(): lax.psum(jnp.dot(activated, out_weight, preferred_element_type=jnp.float3...]
    all_gather x0 -> x1, blocking collectives: none -> 6.53 us  [shards(): lax.all_gather(jnp.dot(activated, out_weight, preferred_element_type=jnp....]
where the time goes in v1:
time: 66 us; the launch traced here: 65.3 us
  blocking collectives  25.2 us (38%)
  matrix products  22 us (33%)
  waiting for transfers between devices  5.28 us (8%)
  other arithmetic  5 us (8%)
  local copies, waits for them, and re-layouts  3.84 us (6%)
  starting transfers between devices  3.33 us (5%)
  between operations  0.72 us (1%)
    all_to_all x1, blocking collectives, shards(): lax.all_to_all(jnp.repeat(outgoing, group_span, axis=0), 'ep', split_axis...  12.9 us
    all_gather x1, blocking collectives, shards(): lax.all_gather(jnp.dot(activated, out_weight, preferred_element_type=jnp....  6.53 us
    all_gather x1, blocking collectives, shards(): lax.all_gather(hidden, 'tp', axis=1, tiled=True)  5.77 us
    all_to_all x1, waiting for transfers between devices, shards(): lax.all_to_all(rounded, 'ep', split_axis=0, concat_axis=0, tiled=True)  5.28 us
    dot_general x1, matrix products, shards(): up_pre = jnp.dot(slot_rows, up_weight, preferred_element_type=jnp.float32)  4.58 us
    dot_general x1, matrix products, shards(): jnp.dot(slot_rows, gate_weight, preferred_element_type=jnp.float32)  4.58 us
    dot_general x1, matrix products, shards(): jnp.dot(lax.all_gather(hidden, 'tp', axis=1, tiled=True), down_weight, pr...  4.56 us
    all_to_all x1, starting transfers between devices, shards(): lax.all_to_all(rounded, 'ep', split_axis=0, concat_axis=0, tiled=True)  3.33 us
  transfers between devices with their start and end apart: 1, of which 1 were waited for; matrix products, arithmetic and copies ran while one was open for 2% of the time, Pallas kernels for 0%

profile of v1, /device:TPU:0, one launch (start us, length us, event | category | flops | bytes accessed | tf_op | source)
XLA Modules:
  0.0 65.3 jit_solution(859107882188646898)
XLA Ops:
  0.6 0.0 copy-start
  0.7 0.8 %constant_dynamic-slice_fusion = s32[4,2]{0,1:T(2,128)S(1)} fusion(s32[32,2]{0,1:T(2,128)} %param.35, s32[]{:T(128)S(6)} %select_n.14), kind=kLoop, calls=%fused_computation.78 | loop fusion | bytes 68 | tf_op jit(solution)/shard_map/dynamic_slice | solution.py:125
  1.5 0.1 copy.71
  1.6 0.1 eq.56
  1.7 0.1 fusion.42
  1.7 0.7 %exp.10 = f32[16]{0:T(128)S(1)} exponential(f32[16]{0:T(128)} %param.25) | non-fusion elementwise | bytes 128 | tf_op jit(solution)/shard_map/exp | solution.py:20
  2.4 0.9 %fusion.19 = f32[4]{0:T(128)S(1)} fusion(bf16[4,2048]{1,0:T(4,128)(2,1)} %param.20), kind=kLoop, calls=%fused_computation.33 | loop fusion | flops 24572 | bytes 16400 | tf_op jit(solution)/shard_map/reduce_sum | solution.py:14
  3.3 0.7 %convert_element_type.68 = f32[2048]{0:T(1024)S(1)} convert(bf16[2048]{0:T(1024)(128)(2,1)} %param.21) | non-fusion elementwise | flops 2048 | bytes 12288 | tf_op jit(solution)/shard_map/convert_element_type | solution.py:15
  4.0 1.5 %convolution_convert_fusion.2 = bf16[4,256]{1,0:T(4,128)(2,1)S(1)} fusion(bf16[2048,256]{1,0:T(8,128)(2,1)} %param.22, bf16[4,2048]{1,0:T(4,128)(2,1)} %param.20, f32[2048]{0:T(1024)S(1)} %convert_element_type.68, f32[4]{0:T(128)S(1)} %add_rsqrt_fusion.1), kind=kOutput, calls=%fused_computation.14 | convolution fusion | flops 4228096 | bytes 1075216 | tf_op jit(solution)/shard_map/dot_general | solution.py:99
  5.5 0.1 reshape.72
  5.6 0.8 %cosine_multiply_fusion = (f32[16,64]{1,0:T(8,128)S(1)}, f32[16,64]{1,0:T(8,128)S(1)}, f32[16,64]{1,0:T(8,128)S(1)}, f32[16,64]{1,0:T(8,128)S(1)}) fusion(f32[16,64]{1,0:T(8,128)} %param.24, f32[16,64]{1,0:T(8,128)} %param.23, f32[16]{0:T(128)S(1)} %exp.10), kind=kLoop, calls=%fused_computation.52 | loop fusion | flops 17408 | bytes 24640 | tf_op jit(solution)/shard_map/mul | solution.py:24
  6.4 1.2 %fusion.2 = f32[4,16,64]{2,0,1:T(4,128)S(1)} fusion(f32[16,64,16]{1,2,0:T(8,128)} %param.26, f32[16,64,16]{1,2,0:T(8,128)} %param.27, f32[16,64]{1,0:T(8,128)S(1)} %get-tuple-element.21, f32[16,64]{1,0:T(8,128)S(1)} %get-tuple-element.20, f32[4,16,64]{2,1,0:T(8,128)} %param.32, f32[4,16,64]{2,1,0:T(8,128)} %param.31, f32[16,64]{1,0:T(8,128)S(1)} %get-tuple-element.22, ...), kind=kOutput, calls=%fused_computation.7 | convolution fusion | flops 851968 | bytes 198656 | tf_op jit(solution)/shard_map/sgp,gnp->sgn/dot_general | solution.py:55
  7.6 1.2 %fusion.3 = f32[4,16,64]{2,0,1:T(4,128)S(1)} fusion(f32[16,64,16]{1,2,0:T(8,128)} %param.27, f32[16,64,16]{1,2,0:T(8,128)} %param.26, f32[16,64]{1,0:T(8,128)S(1)} %get-tuple-element.21, f32[16,64]{1,0:T(8,128)S(1)} %get-tuple-element.20, f32[4,16,64]{2,1,0:T(8,128)} %param.32, f32[4,16,64]{2,1,0:T(8,128)} %param.31, f32[16,64]{1,0:T(8,128)S(1)} %get-tuple-element.22, ...), kind=kOutput, calls=%fused_computation.9 | convolution fusion | flops 851968 | bytes 198656 | tf_op jit(solution)/shard_map/sgp,gnp->sgn/dot_general | solution.py:54
  8.8 0.1 fusion.45
  8.9 0.1 fusion.43
  9.0 0.7 %convert_element_type.80 = f32[2048]{0:T(1024)S(1)} convert(bf16[2048]{0:T(1024)(128)(2,1)} %param.34) | non-fusion elementwise | flops 2048 | bytes 12288 | tf_op jit(solution)/shard_map/convert_element_type | solution.py:15
  9.7 1.2 %fusion.59 = f32[16,4,16]{2,1,0:T(4,128)S(1)} fusion(f32[4,16,64]{2,0,1:T(4,128)S(1)} %fusion.3, f32[16,16,64]{2,1,0:T(8,128)} %param.28), kind=kOutput, calls=%fused_computation.84 | convolution fusion | flops 786432 | bytes 86016 | tf_op jit(solution)/shard_map/sgn,gpn->sgp/dot_general | solution.py:58
  10.9 1.2 %fusion.1 = f32[4,16,16]{2,0,1:T(4,128)S(1)} fusion(f32[16,4,16]{2,1,0:T(4,128)S(1)} %fusion.59, f32[4,16,64]{2,0,1:T(4,128)S(1)} %fusion.2, f32[16,16,64]{2,1,0:T(8,128)} %param.29), kind=kOutput, calls=%fused_computation.5 | convolution fusion | flops 787456 | bytes 90112 | tf_op jit(solution)/shard_map/sgn,gpn->sgp/dot_general | solution.py:58
  12.1 0.1 reshape.73
  12.2 0.0 copy-done
  12.2 0.9 %convolution_bitcast_fusion = f32[1,4,2048]{2,1,0:T(4,128)S(1)} fusion(bf16[256,2048]{1,0:T(8,128)(2,1)S(1)} %copy-done, f32[4,256]{1,0:T(4,128)S(1)} %reshape.73, bf16[4,256]{1,0:T(4,128)(2,1)S(1)} %convolution_convert_fusion.2, f32[256]{0:T(256)} %param.30), kind=kOutput, calls=%fused_computation.3 | convolution fusion | flops 4206592 | bytes 1088512 | tf_op jit(solution)/shard_map/dot_general | solution.py:116
  13.2 6.5 %all-gather.1 = f32[4,4,2048]{2,1,0:T(4,128)S(1)} all-gather(f32[1,4,2048]{2,1,0:T(4,128)S(1)} %convolution_bitcast_fusion), channel_id=2, replica_groups=mesh['ep'=8,'tp'=4] {'tp'}, dimensions={0}, use_global_device_ids=true | all-gather | bytes 163840 | tf_op jit(solution)/shard_map/all_gather | solution.py:116
  19.7 0.9 %fusion.16 = (f32[4]{0:T(128)S(1)}, bf16[4,2048]{1,0:T(4,128)(2,1)S(1)}) fusion(f32[4,2048]{1,0:T(4,128)S(1)} %reduce_sum.50, bf16[4,2048]{1,0:T(4,128)(2,1)} %param.20), kind=kLoop, calls=%fused_computation.30 | loop fusion | flops 49148 | bytes 65552 | tf_op jit(solution)/shard_map/reduce_sum | solution.py:14
  20.6 0.8 %select_reduce_fusion.1 = (f32[4,8,2]{1,0,2:T(4,128)S(1)}, bf16[4,8,2]{1,0,2:T(4,128)(2,1)S(1)}) fusion(f32[4,2]{0,1:T(2,128)} %param.36, s32[4,2,8]{2,0,1:T(4,128)S(1)} %copy.73, pred[4,2,8]{2,0,1:T(4,128)(4,1)S(1)} %copy.74), kind=kLoop, calls=%fused_computation.46 | loop fusion | flops 640 | bytes 736 | tf_op jit(solution)/shard_map/reduce_sum | solution.py:72
  21.3 0.2 convolution_convert_fusion
  21.6 0.1 copy.75
  21.6 12.9 %all_to_all.10 = bf16[8,2,2048]{2,1,0:T(2,128)(2,1)S(1)} all-to-all(bf16[8,2,2048]{2,1,0:T(2,128)(2,1)S(1)} %copy.75), channel_id=1, replica_groups=mesh['ep'=8,'tp'=4] {'ep'}, dimensions={0} | all-to-all | bytes 131072 | tf_op jit(solution)/shard_map/all_to_all | solution.py:131
  34.5 4.6 %fusion.60 = f32[16,2048]{1,0:T(8,128)S(1)} fusion(bf16[16,2048]{1,0:T(8,128)(2,1)S(1)} %reshape.74, bf16[2048,2048]{1,0:T(8,128)(2,1)} %param.37), kind=kOutput, calls=%fused_computation.85 | convolution fusion | flops 134217728 | bytes 8585216 | tf_op jit(solution)/shard_map/dot_general | solution.py:135
  39.1 4.6 %fusion = bf16[16,2048]{1,0:T(8,128)(2,1)S(1)} fusion(bf16[16,2048]{1,0:T(8,128)(2,1)S(1)} %reshape.74, bf16[2048,2048]{1,0:T(8,128)(2,1)} %param.38, f32[16,2048]{1,0:T(8,128)S(1)} %fusion.60), kind=kOutput, calls=%fused_computation.2 | convolution fusion | flops 134414336 | bytes 8650752 | tf_op jit(solution)/shard_map/dot_general | solution.py:136
  43.7 5.8 %all_gather.11 = bf16[16,8192]{1,0:T(8,128)(2,1)S(1)} all-gather(bf16[16,2048]{1,0:T(8,128)(2,1)S(1)} %fusion), channel_id=1, replica_groups=mesh['ep'=8,'tp'=4] {'tp'}, dimensions={1}, use_global_device_ids=true | all-gather | bytes 327680 | tf_op jit(solution)/shard_map/all_gather | solution.py:140
  49.5 4.6 %convolution_convert_fusion.1 = bf16[16,512]{1,0:T(8,128)(2,1)S(1)} fusion(bf16[16,8192]{1,0:T(8,128)(2,1)S(1)} %all_gather.11, bf16[8192,512]{1,0:T(8,128)(2,1)} %param.39), kind=kOutput, calls=%fused_computation.10 | convolution fusion | flops 134225920 | bytes 8667136 | tf_op jit(solution)/shard_map/dot_general | solution.py:139
  54.0 0.6 reshape.75
  54.7 3.3 %all-to-all-start.1 = ((bf16[8,2,512]{2,1,0:T(2,128)(2,1)}), bf16[8,2,512]{2,1,0:T(2,128)(2,1)S(1)}, u32[]{:S(2)}, u32[]{:S(2)}) async-start(bf16[8,2,512]{2,1,0:T(2,128)(2,1)} %reshape.75), calls=%async_computation.1 | async-start | bytes 32768 | tf_op jit(solution)/shard_map/all_to_all | solution.py:145
  58.0 0.6 copy.77
  58.6 0.6 copy.78
  59.2 5.3 %all-to-all-done.1 = bf16[8,2,512]{2,1,0:T(2,128)(2,1)S(1)} async-done(((bf16[8,2,512]{2,1,0:T(2,128)(2,1)}), bf16[8,2,512]{2,1,0:T(2,128)(2,1)S(1)}, u32[]{:S(2)}, u32[]{:S(2)}) %all-to-all-start.1) | async-done | bytes 16416 | tf_op jit(solution)/shard_map/all_to_all | solution.py:145
  64.5 0.8 %fusion.5 = bf16[4,512]{1,0:T(4,128)(2,1)} fusion(bf16[8,2,512]{2,1,0:T(2,128)(2,1)S(1)} %all-to-all-done.1, f32[4,8,2]{1,0,2:T(4,128)S(1)} %get-tuple-element.15, bf16[4,2048]{1,0:T(4,128)(2,1)S(1)} %get-tuple-element.18, s32[]{:T(128)S(6)} %select_n.13), kind=kOutput, calls=%fused_computation.13 | convolution fusion | flops 399360 | bytes 24836 | tf_op jit(solution)/shard_map/xcs,xcd->sd/dot_general | solution.py:150
  (8 shorter events, 0.1 us)
Async XLA Ops:
  0.6 11.6 %copy-start = (bf16[256,2048]{1,0:T(8,128)(2,1)S(1)}, bf16[256,2048]{1,0:T(8,128)(2,1)}, u32[]{:S(2)}) copy-start(bf16[256,2048]{1,0:T(8,128)(2,1)} %param.33) | copy-start | bytes 3145732
  54.7 9.9 %all-to-all-start.1 = ((bf16[8,2,512]{2,1,0:T(2,128)(2,1)}), bf16[8,2,512]{2,1,0:T(2,128)(2,1)S(1)}, u32[]{:S(2)}, u32[]{:S(2)}) async-start(bf16[8,2,512]{2,1,0:T(2,128)(2,1)} %reshape.75), calls=%async_computation.1 | async-start | bytes 32768 | tf_op jit(solution)/shard_map/all_to_all | solution.py:145
